TPU v7x, 512 devices: a whole 4x4x16 slice. The times are simulated.
512 devices in a mesh: sp: 32 (over z, core), tp: 16 (over y, x).
Axes of the slice: x: 4, y: 4, z: 16, core: 2. Of those that a mesh axis runs over, the one named last changes fastest.
Arguments:
- layer_input: bfloat16 [8, 4096, 2048], P(None, 'sp', 'tp'), may hold values from -6 to 6
- w_key: bfloat16 [2048, 2048], P(None, 'tp'), may hold values from -0.125 to 0.125
- w_value: bfloat16 [2048, 2048], P(None, 'tp'), may hold values from -0.125 to 0.125
- w_gates: bfloat16 [2, 2048, 16], replicated, may hold values from -0.125 to 0.125
- decay_rate: float32 [16], P('tp'), may hold values from 0 to 1, as said below
- beta_bias: float32 [16], P('tp'), may hold values from -5.5 to -3
- log_decay_extra: float32 [8, 16, 4096], P(None, 'tp', 'sp'), may hold values from -2 to 0, as said below
- new_query: bfloat16 [8, 2048], P(None, 'tp'), may hold values from -6 to 6
- read_gain: float32 [128], replicated, may hold values from 0.1 to 1.9
Outputs:
- state_cache: bfloat16 [1024, 2048], P('sp', 'tp')
- first_read: bfloat16 [8, 2048], P(None, 'tp')
Inputs may be any that keep to these rules, and one draw needn't show every extreme that they name: `decay_rate`: a positive rate for each head. `log_decay_extra`: additions that are never positive.
All inputs are finite; a program needn't handle non-finite values.
Results may differ from a plain program's by a relative error of at most 0.0052.
Values may be sent and summed in bfloat16 or wider, within the bound.
No kernel may reach another device: no remote copies, remote signals or barrier semaphores. Data moves between devices by JAX's collectives and lax.ppermute only.
A program may use at most 64 MiB of HBM per device.

v0:
```python
import jax
import jax.numpy as jnp
from jax import lax
from jax.sharding import Mesh
from jax.sharding import PartitionSpec as P

DK = 128
DV = 128
BLOCK = 64
SP = ("sp_0", "sp_1")
EPS = 1e-06
HIGH = lax.Precision.HIGHEST


def nothing_yet(x, identity):
    return jnp.broadcast_to(jnp.asarray(identity, x.dtype), x.shape)


def prefix_by_axis(x, axes, combine, identity):
    before = start = nothing_yet(x, identity)
    total = x
    for axis in reversed(axes):
        count, position = (lax.axis_size(axis), lax.axis_index(axis))
        pieces = lax.all_gather(total, axis)
        inside, total = (start, start)
        for k in reversed(range(count)):
            passed = k > position
            total = combine(total, pieces[k])
            inside = jnp.where(passed, total, inside)
        before = combine(inside, before)
    return before


def cut_along(x, dim, count):
    shape = x.shape
    pieces = x.reshape(*shape[:dim], count, shape[dim] // count, *shape[dim + 1 :])
    return jnp.moveaxis(pieces, dim, 0)


def summed_on_arrival(x, axis, dim):
    pieces = cut_along(x, dim, lax.axis_size(axis))
    arrived = lax.all_to_all(pieces, axis, split_axis=0, concat_axis=0, tiled=True)
    return arrived.sum(axis=0)


def sent_to_all(x, axis):
    count = lax.axis_size(axis)
    return lax.all_to_all(jnp.broadcast_to(x[None], (count, *x.shape)), axis, 0, 0, tiled=True)


def taken_together(x, axis):
    return sent_to_all(x, axis).sum(axis=0)


def unit_rows(values):
    return values * lax.rsqrt(jnp.sum(values * values, axis=-1, keepdims=True) + EPS)


def matmul_high(left, right):
    return jnp.einsum("...ab,...bc->...ac", left, right, precision=HIGH)


def block_pieces(keys, values, log_decay, beta):
    size = keys.shape[-2]
    width = values.shape[-1]
    running = jnp.cumsum(log_decay, axis=-1)
    sequence_indices = jnp.arange(size)
    causal = sequence_indices[:, None] >= sequence_indices[None, :]
    strict = sequence_indices[:, None] > sequence_indices[None, :]
    spread = running[..., :, None] - running[..., None, :]
    weights = jnp.where(causal, jnp.exp(jnp.where(causal, spread, 0.0)), 0.0)
    key_beta = keys * beta[..., None]
    lower = jnp.where(
        strict, jnp.einsum("...cd,...sd->...cs", key_beta, keys, precision=HIGH) * weights, 0.0
    )
    right_side = jnp.concatenate(
        [values * beta[..., None], key_beta * jnp.exp(running)[..., None]], axis=-1
    )
    solved = lax.linalg.triangular_solve(
        lower, right_side, left_side=True, lower=True, unit_diagonal=True
    )
    fresh = solved[..., :width]
    erase = solved[..., width:]
    last = running[..., -1]
    key_late = keys * jnp.exp(last[..., None] - running)[..., None]
    identity = jnp.eye(keys.shape[-1], dtype=jnp.float32)
    transition = jnp.exp(last)[..., None, None] * identity - jnp.einsum(
        "...cd,...ce->...de", key_late, erase, precision=HIGH
    )
    inject = jnp.einsum("...cd,...cv->...dv", key_late, fresh, precision=HIGH)
    return (transition, inject)


def shards(
    layer_input,
    w_key,
    w_value,
    w_gates,
    decay_rate,
    beta_bias,
    log_decay_extra,
    new_query,
    read_gain,
):
    prompts, seg_len, _ = layer_input.shape
    heads_here = w_key.shape[1] // DK
    blocks = seg_len // BLOCK
    first_head = lax.axis_index("tp") * heads_here
    gate_cols = lax.dynamic_slice_in_dim(w_gates, first_head, heads_here, 2)
    joined = jnp.concatenate([w_key, w_value], axis=1)
    piece = lax.all_gather(layer_input, "tp", axis=2, tiled=True)
    pair_sum = jnp.einsum("std,de->ste", piece, joined, preferred_element_type=jnp.float32)
    gate_sum = jnp.einsum("std,gdh->gsth", piece, gate_cols, preferred_element_type=jnp.float32)
    key_pre = pair_sum[..., : heads_here * DK].reshape(prompts, seg_len, heads_here, DK)
    value_pre = pair_sum[..., heads_here * DK :].reshape(prompts, seg_len, heads_here, DV)
    keys = unit_rows(jax.nn.silu(key_pre))
    values = jax.nn.silu(value_pre)
    log_decay = -decay_rate * jax.nn.softplus(gate_sum[0]) + log_decay_extra.transpose(0, 2, 1)
    beta = jax.nn.sigmoid(gate_sum[1] + beta_bias)
    key_blocks = keys.reshape(prompts, blocks, BLOCK, heads_here, DK).transpose(0, 3, 1, 2, 4)
    value_tiles = values.reshape(prompts, blocks, BLOCK, heads_here, DV).transpose(0, 3, 1, 2, 4)
    decay_blocks = log_decay.reshape(prompts, blocks, BLOCK, heads_here).transpose(0, 3, 1, 2)
    strength_groups = beta.reshape(prompts, blocks, BLOCK, heads_here).transpose(0, 3, 1, 2)
    transition, inject = block_pieces(key_blocks, value_tiles, decay_blocks, strength_groups)

    def compose_maps(carry, piece):
        total_map, total_add = carry
        block_map, block_add = piece
        return (
            (matmul_high(block_map, total_map), matmul_high(block_map, total_add) + block_add),
            None,
        )

    identity = jnp.eye(DK, dtype=jnp.float32)
    map_start = jnp.broadcast_to(identity, (prompts, heads_here, DK, DK))
    add_start = jnp.zeros((prompts, heads_here, DK, DV), jnp.float32)
    (seg_map, seg_add), _ = lax.scan(
        compose_maps,
        (map_start, add_start),
        (jnp.moveaxis(transition, 2, 0), jnp.moveaxis(inject, 2, 0)),
    )
    local_rows = prompts * DK // lax.axis_size(SP)
    leading_line = lax.axis_index(SP) * local_rows
    query = new_query.reshape(prompts, heads_here, DK)

    def later_first(earlier, later):
        return matmul_high(earlier, later)

    after = prefix_by_axis(seg_map, SP, later_first, map_start)
    term = jnp.einsum("shab,shbv->sahv", after, seg_add, precision=HIGH).reshape(
        prompts * DK, heads_here * DV
    )
    owned = summed_on_arrival(term, SP, 0)
    state_cache = owned.astype(jnp.bfloat16)
    query_rows = query.transpose(0, 2, 1).reshape(prompts * DK, heads_here)
    my_query = lax.dynamic_slice_in_dim(query_rows, leading_line, local_rows, 0)
    owner = (leading_line + jnp.arange(local_rows)) // DK
    member = (owner[:, None] == jnp.arange(prompts)[None, :]).astype(jnp.float32)
    weighted = my_query.astype(jnp.float32)[:, :, None] * state_cache.reshape(
        local_rows, heads_here, DV
    ).astype(jnp.float32)
    partial_read = jnp.einsum("rs,rhv->shv", member, weighted, precision=HIGH)
    raw_read = taken_together(partial_read, SP)
    scaled = (
        raw_read
        * lax.rsqrt(jnp.mean(raw_read * raw_read, axis=-1, keepdims=True) + EPS)
        * read_gain
    )
    first_read = scaled.astype(jnp.bfloat16).reshape(prompts, heads_here * DV)
    return (state_cache, first_read)


def solution(mesh):
    finer = Mesh(mesh.devices.reshape(16, 2, mesh.shape["tp"]), ("sp_0", "sp_1", "tp"))
    placed = (
        P(None, SP, "tp"),
        P(None, "tp"),
        P(None, "tp"),
        P(),
        P("tp"),
        P("tp"),
        P(None, "tp", SP),
        P(None, "tp"),
        P(),
    )
    return jax.shard_map(
        shards, mesh=finer, in_specs=placed, out_specs=(P(SP, "tp"), P(None, "tp")), check_vma=False
    )
```

profile of v0, /device:TPU:1, one launch (start us, length us, event | category | flops | bytes accessed | tf_op | source)
XLA Modules:
  0.0 407.0 jit_solution(17985307926556200827)
XLA Ops:
  7.2 0.7 all-gather.6.cloned.1.call-update
  9.3 0.6 broadcast.269
  9.8 1.4 reduce.14
  11.5 75.6 %all-gather.6.cloned.1.call-done = bf16[8,128,2048]{2,1,0:T(8,128)(2,1)} async-done(((bf16[8,128,128]{2,1,0:T(8,128)(2,1)}), bf16[8,128,2048]{2,1,0:T(8,128)(2,1)}) %all-gather.6.cloned.1.call-update) | async-done | bytes 4194320 | tf_op jit(solution)/shard_map/all_gather | solution.py:111
  87.1 3.4 fusion.75
  90.6 0.5 reduce_window_sum.13
  91.4 3.8 convolution_bitcast_fusion.2
  95.4 0.3 divide_multiply_fusion
  95.8 1.1 fusion.13
  96.9 78.6 %custom-call.3 = f32[8,1,2,1,64,64]{4,5,3,2,1,0:T(8,128)S(1)} custom-call(f32[8,1,2,1,64,64]{5,4,3,2,1,0:T(8,128)S(1)} %fusion.13), custom_call_target="InvertDiagBlocksLowerTriangular" | custom-call | tf_op jit(solution)/shard_map/triangular_solve | solution.py:79
  175.5 0.4 broadcast_multiply_fusion
  175.9 1.1 convolution_bitcast_fusion.3
  176.9 2.0 convolution_bitcast_fusion.1
  178.9 2.0 fusion.9
  181.0 2.8 while.12
  181.1 0.6 fusion.114
  181.8 0.6 convolution_bitcast_fusion.5
  182.5 0.6 fusion.114
  183.2 0.6 convolution_bitcast_fusion.5
  183.9 0.8 copy-done.1
  184.9 21.7 %all-gather.8.cloned.1.call-done = f32[16,1,128,128]{3,2,1,0:T(8,128)} async-done(((f32[8,1,128,128]{3,2,1,0:T(8,128)}), f32[16,1,128,128]{3,2,1,0:T(8,128)}) %all-gather.8.cloned.1.call-update) | async-done | bytes 1048592 | tf_op jit(solution)/shard_map/all_gather | solution.py:24
  206.6 1.6 fusion.51
  208.3 2.5 fusion.50
  210.8 0.6 fusion.55
  211.5 105.1 %all-gather.10.cloned.1.call-done = f32[128,128,128]{2,1,0:T(8,128)} async-done(((f32[8,128,128]{2,1,0:T(8,128)}), f32[128,128,128]{2,1,0:T(8,128)}) %all-gather.10.cloned.1.call-update) | async-done | bytes 8388624 | tf_op jit(solution)/shard_map/all_gather | solution.py:24
  316.6 1.8 fusion.48
  318.3 2.1 fusion.46
  320.5 1.7 fusion.44
  322.2 1.7 fusion.42
  323.9 1.7 fusion.40
  325.6 1.7 fusion.38
  327.2 0.7 fusion.36
  327.9 0.7 fusion.34
  328.6 0.7 fusion.32
  329.3 0.7 fusion.30
  329.9 0.7 fusion.28
  330.6 0.7 fusion.26
  331.3 0.7 fusion.24
  332.0 0.7 fusion.22
  332.6 0.7 fusion.20
  333.3 1.3 convolution_select_fusion
  334.6 0.6 fusion.82
  335.2 1.4 fusion.52
  336.7 9.8 %all-to-all-start = ((f32[32,32,128]{2,1,0:T(8,128)}), f32[32,32,128]{2,1,0:T(8,128)S(1)}, u32[]{:S(2)}, u32[]{:S(2)}) async-start(f32[32,32,128]{2,1,0:T(8,128)} %bitcast.32), calls=%async_computation | async-start | bytes 1048576 | tf_op jit(solution)/shard_map/all_to_all | solution.py:42
  346.6 33.4 %all-to-all-done = f32[32,32,128]{2,1,0:T(8,128)S(1)} async-done(((f32[32,32,128]{2,1,0:T(8,128)}), f32[32,32,128]{2,1,0:T(8,128)S(1)}, u32[]{:S(2)}, u32[]{:S(2)}) %all-to-all-start) | async-done | bytes 524320 | tf_op jit(solution)/shard_map/all_to_all | solution.py:42
  380.0 0.3 fusion.70
  380.3 19.3 %all_to_all.10 = f32[32,8,1,128]{3,1,2,0:T(8,128)S(1)} all-to-all(f32[32,8,1,128]{3,1,2,0:T(8,128)S(1)} %broadcast_in_dim.27), channel_id=1, replica_groups=mesh['sp_0'=16,'sp_1'=2,'tp'=16] {'sp_0','sp_1'}, dimensions={0} | all-to-all | bytes 262144 | tf_op jit(solution)/shard_map/all_to_all | solution.py:48
  399.8 0.7 multiply_convert_fusion
  (50 shorter events, 1.9 us)
Async XLA Ops:
  7.2 4.2 %copy-start = (bf16[2,2048,16]{1,2,0:T(8,128)(2,1)S(1)}, bf16[2,2048,16]{1,2,0:T(8,128)(2,1)}, u32[]{:S(2)}) copy-start(bf16[2,2048,16]{1,2,0:T(8,128)(2,1)} %param.14) | copy-start | bytes 393220
  7.2 79.9 %all-gather.6.cloned.1.call-start = ((), (), s32[]{:S(2)}) async-start(), calls=%async_computation.2 | async-start | bytes 4456448 | tf_op jit(solution)/shard_map/all_gather | solution.py:111
  7.9 198.7 %all-gather.8.cloned.1.call-start = ((), (), s32[]{:S(2)}) async-start(), calls=%async_computation.3 | async-start | bytes 1572864 | tf_op jit(solution)/shard_map/all_gather | solution.py:24
  183.9 0.8 copy-start.1
  184.7 131.9 %all-gather.10.cloned.1.call-start = ((), (), s32[]{:S(2)}) async-start(), calls=%async_computation.4 | async-start | bytes 8912896 | tf_op jit(solution)/shard_map/all_gather | solution.py:24
  316.6 10.7 %copy-start.2 = (f32[128,128,128]{2,1,0:T(8,128)S(1)}, f32[128,128,128]{2,1,0:T(8,128)}, u32[]{:S(2)}) copy-start(f32[128,128,128]{2,1,0:T(8,128)} %all-gather.10.cloned.1.call-done) | copy-start | bytes 25165828
  331.9 14.5 %copy-start.4 = (bf16[8,128]{1,0:T(8,128)(2,1)S(1)}, bf16[8,128]{1,0:T(8,128)(2,1)}, u32[]{:S(2)}) copy-start(bf16[8,128]{1,0:T(8,128)(2,1)} %param.18) | copy-start | bytes 6148
  331.9 67.8 %copy-start.5 = (f32[128]{0:T(128)S(1)}, f32[128]{0:T(128)}, u32[]{:S(2)}) copy-start(f32[128]{0:T(128)} %param.19) | copy-start | bytes 1540
  336.7 43.3 %all-to-all-start = ((f32[32,32,128]{2,1,0:T(8,128)}), f32[32,32,128]{2,1,0:T(8,128)S(1)}, u32[]{:S(2)}, u32[]{:S(2)}) async-start(f32[32,32,128]{2,1,0:T(8,128)} %bitcast.32), calls=%async_computation | async-start | bytes 1048576 | tf_op jit(solution)/shard_map/all_to_all | solution.py:42
  380.0 20.4 %copy-start.3 = (bf16[32,128]{1,0:T(8,128)(2,1)}, bf16[32,128]{1,0:T(8,128)(2,1)S(1)}, u32[]{:S(2)}) copy-start(bf16[32,128]{1,0:T(8,128)(2,1)S(1)} %reduce_sum.37) | copy-start | bytes 24580
Sparse Core Ops, SparseCore 0:
  11.0 76.0 all-gather.5
  184.8 21.7 all-gather.7
  210.9 105.5 all-gather.9
where the time goes:
time: 408 us; the launch traced here: 407 us
  waiting for transfers between devices  236 us (58%)
  other arithmetic  82.5 us (20%)
  matrix products  40.8 us (10%)
  blocking collectives  19.3 us (5%)
  between operations  15.5 us (4%)
  starting transfers between devices  10.1 us (2%)
    all_gather x2, waiting for transfers between devices, prefix_by_axis(): pieces = lax.all_gather(total, axis)  127 us
    another operation x3, other arithmetic, block_pieces(): lax.linalg.triangular_solve(lower, right_side, left_side=True, lower=True...  78.7 us
    all_gather x1, waiting for transfers between devices, shards(): piece = lax.all_gather(layer_input, 'tp', axis=2, tiled=True)  75.6 us
    all_to_all x1, waiting for transfers between devices, summed_on_arrival(): lax.all_to_all(pieces, axis, split_axis=0, concat_axis=0, tiled=True)  33.4 us
    dot_general x24, matrix products, matmul_high(): return jnp.einsum('...ab,...bc->...ac', left, right, precision=HIGH)  25.9 us
    all_to_all x1, blocking collectives, sent_to_all(): lax.all_to_all(jnp.broadcast_to(x[None], (count, *x.shape)), axis, 0, 0,...  19.3 us
    all_to_all x1, starting transfers between devices, summed_on_arrival(): lax.all_to_all(pieces, axis, split_axis=0, concat_axis=0, tiled=True)  9.76 us
  transfers between devices with their start and end apart: 4, of which 4 were waited for; matrix products, arithmetic and copies ran while one was open for 1% of the time, Pallas kernels for 0%

commit v1 on v0

--- a/solution.py
+++ b/solution.py
@@ -108,7 +108,11 @@
     first_head = lax.axis_index("tp") * heads_here
     gate_cols = lax.dynamic_slice_in_dim(w_gates, first_head, heads_here, 2)
     joined = jnp.concatenate([w_key, w_value], axis=1)
-    piece = lax.all_gather(layer_input, "tp", axis=2, tiled=True)
+    panels = []
+    for _ in range(lax.axis_size("tp")):
+        panels.append(layer_input)
+    even = lax.all_to_all(jnp.stack(panels), "tp", 0, 0)
+    piece = jnp.concatenate(even, 2)
     pair_sum = jnp.einsum("std,de->ste", piece, joined, preferred_element_type=jnp.float32)
     gate_sum = jnp.einsum("std,gdh->gsth", piece, gate_cols, preferred_element_type=jnp.float32)
     key_pre = pair_sum[..., : heads_here * DK].reshape(prompts, seg_len, heads_here, DK)

time: 408 us -> 404 us (level)
  waiting for transfers between devices: 236 us -> 222 us
  starting transfers between devices: 10.1 us -> 17.6 us
    all_gather x1 -> x0, waiting for transfers between devices: 75.6 us -> none  [shards(): piece = lax.all_gather(layer_input, 'tp', axis=2, tiled=True)]
    all_to_all x0 -> x1, waiting for transfers between devices: none -> 51.2 us  [shards(): even = lax.all_to_all(jnp.stack(panels), 'tp', 0, 0)]
    all_gather x2, waiting for transfers between devices: 127 us -> 138 us  [prefix_by_axis(): pieces = lax.all_gather(total, axis)]
    all_to_all x0 -> x1, starting transfers between devices: none -> 7.62 us  [shards(): even = lax.all_to_all(jnp.stack(panels), 'tp', 0, 0)]
  transfers between devices with their start and end apart: 4 -> 4, of which waited for: 4 -> 4; matrix products, arithmetic and copies ran while one was open for 1% -> 0% of each run, Pallas kernels for 0% -> 0%
where the time goes in v1:
time: 404 us
  waiting for transfers between devices  222 us (55%)
  other arithmetic  81.7 us (20%)
  matrix products  40.5 us (10%)
  blocking collectives  19.3 us (5%)
  starting transfers between devices  17.6 us (4%)
  between operations  15.8 us (4%)
  local copies, waits for them, and re-layouts  6.18 us (2%)
    all_gather x2, waiting for transfers between devices, prefix_by_axis(): pieces = lax.all_gather(total, axis)  138 us
    another operation x3, other arithmetic, block_pieces(): lax.linalg.triangular_solve(lower, right_side, left_side=True, lower=True...  78.7 us
    all_to_all x1, waiting for transfers between devices, shards(): even = lax.all_to_all(jnp.stack(panels), 'tp', 0, 0)  51.2 us
    all_to_all x1, waiting for transfers between devices, summed_on_arrival(): lax.all_to_all(pieces, axis, split_axis=0, concat_axis=0, tiled=True)  33.4 us
    dot_general x24, matrix products, matmul_high(): return jnp.einsum('...ab,...bc->...ac', left, right, precision=HIGH)  25.9 us
    all_to_all x1, blocking collectives, sent_to_all(): lax.all_to_all(jnp.broadcast_to(x[None], (count, *x.shape)), axis, 0, 0,...  19.3 us
    all_to_all x1, starting transfers between devices, summed_on_arrival(): lax.all_to_all(pieces, axis, split_axis=0, concat_axis=0, tiled=True)  9.76 us
  transfers between devices with their start and end apart: 4, of which 4 were waited for; matrix products, arithmetic and copies ran while one was open for 0% of the time, Pallas kernels for 0%

profile of v1, /device:TPU:1, one launch (start us, length us, event | category | flops | bytes accessed | tf_op | source)
XLA Modules:
  0.0 403.7 jit_solution(4428323477088397952)
XLA Ops:
  7.2 4.1 %stack.2 = bf16[16,8,128,128]{3,2,1,0:T(8,128)(2,1)} broadcast(bf16[8,128,128]{2,1,0:T(8,128)(2,1)} %param.11), dimensions={1,2,3} | broadcast | bytes 4456448 | tf_op jit(solution)/shard_map/stack | solution.py:114
  11.3 7.6 %all-to-all-start = ((bf16[16,8,128,128]{3,2,1,0:T(8,128)(2,1)}), bf16[16,8,128,128]{3,2,1,0:T(8,128)(2,1)}, u32[]{:S(2)}, u32[]{:S(2)}) async-start(bf16[16,8,128,128]{3,2,1,0:T(8,128)(2,1)} %stack.2), calls=%async_computation | async-start | bytes 8388608 | tf_op jit(solution)/shard_map/all_to_all | solution.py:114
  20.3 0.5 broadcast.271
  20.7 0.6 reduce.14
  21.6 51.2 %all-to-all-done = bf16[16,8,128,128]{3,2,1,0:T(8,128)(2,1)} async-done(((bf16[16,8,128,128]{3,2,1,0:T(8,128)(2,1)}), bf16[16,8,128,128]{3,2,1,0:T(8,128)(2,1)}, u32[]{:S(2)}, u32[]{:S(2)}) %all-to-all-start) | async-done | bytes 4194336 | tf_op jit(solution)/shard_map/all_to_all | solution.py:114
  72.8 3.4 fusion.11
  76.3 0.5 reduce_window_sum.13
  77.1 3.4 fusion.15
  80.8 0.3 divide_multiply_fusion
  81.2 1.1 fusion.22
  82.2 78.6 %custom-call.3 = f32[8,1,2,1,64,64]{4,5,3,2,1,0:T(8,128)S(1)} custom-call(f32[8,1,2,1,64,64]{5,4,3,2,1,0:T(8,128)S(1)} %fusion.22), custom_call_target="InvertDiagBlocksLowerTriangular" | custom-call | tf_op jit(solution)/shard_map/triangular_solve | solution.py:79
  160.9 0.4 broadcast_multiply_fusion
  161.3 1.1 convolution_bitcast_fusion.2
  162.4 2.0 convolution_bitcast_fusion.1
  164.4 2.0 fusion.18
  166.5 2.8 while.12
  166.6 0.6 fusion.122
  167.2 0.6 convolution_bitcast_fusion.4
  168.0 0.6 fusion.122
  168.6 0.6 convolution_bitcast_fusion.4
  169.3 0.8 copy-done.1
  170.4 32.7 %all-gather.5.cloned.1.call-done = f32[16,1,128,128]{3,2,1,0:T(8,128)} async-done(((f32[8,1,128,128]{3,2,1,0:T(8,128)}), f32[16,1,128,128]{3,2,1,0:T(8,128)}) %all-gather.5.cloned.1.call-update) | async-done | bytes 1048592 | tf_op jit(solution)/shard_map/all_gather | solution.py:24
  203.0 1.6 fusion.60
  204.7 2.5 fusion.59
  207.3 0.6 fusion.64
  207.9 105.1 %all-gather.7.cloned.1.call-done = f32[128,128,128]{2,1,0:T(8,128)} async-done(((f32[8,128,128]{2,1,0:T(8,128)}), f32[128,128,128]{2,1,0:T(8,128)}) %all-gather.7.cloned.1.call-update) | async-done | bytes 8388624 | tf_op jit(solution)/shard_map/all_gather | solution.py:24
  313.0 1.8 fusion.57
  314.8 2.1 fusion.55
  316.9 1.7 fusion.53
  318.6 1.7 fusion.51
  320.3 1.7 fusion.49
  322.0 1.7 fusion.47
  323.7 0.7 fusion.45
  324.3 0.7 fusion.43
  325.0 0.7 fusion.41
  325.7 0.7 fusion.39
  326.4 0.7 fusion.37
  327.0 0.7 fusion.35
  327.7 0.7 fusion.33
  328.4 0.7 fusion.31
  329.1 0.7 fusion.29
  329.7 1.3 convolution_select_fusion
  331.0 0.7 fusion.90
  331.7 1.4 fusion.61
  333.1 9.8 %all-to-all-start.1 = ((f32[32,32,128]{2,1,0:T(8,128)}), f32[32,32,128]{2,1,0:T(8,128)S(1)}, u32[]{:S(2)}, u32[]{:S(2)}) async-start(f32[32,32,128]{2,1,0:T(8,128)} %bitcast.33), calls=%async_computation.1 | async-start | bytes 1048576 | tf_op jit(solution)/shard_map/all_to_all | solution.py:42
  343.0 33.4 %all-to-all-done.1 = f32[32,32,128]{2,1,0:T(8,128)S(1)} async-done(((f32[32,32,128]{2,1,0:T(8,128)}), f32[32,32,128]{2,1,0:T(8,128)S(1)}, u32[]{:S(2)}, u32[]{:S(2)}) %all-to-all-start.1) | async-done | bytes 524320 | tf_op jit(solution)/shard_map/all_to_all | solution.py:42
  376.7 19.3 %all_to_all.15 = f32[32,8,1,128]{3,1,2,0:T(8,128)S(1)} all-to-all(f32[32,8,1,128]{3,1,2,0:T(8,128)S(1)} %broadcast_in_dim.27), channel_id=1, replica_groups=mesh['sp_0'=16,'sp_1'=2,'tp'=16] {'sp_0','sp_1'}, dimensions={0} | all-to-all | bytes 262144 | tf_op jit(solution)/shard_map/all_to_all | solution.py:48
  396.2 0.7 multiply_convert_fusion
  (56 shorter events, 2.1 us)
Async XLA Ops:
  7.2 14.3 %copy-start = (bf16[2,2048,16]{1,2,0:T(8,128)(2,1)S(1)}, bf16[2,2048,16]{1,2,0:T(8,128)(2,1)}, u32[]{:S(2)}) copy-start(bf16[2,2048,16]{1,2,0:T(8,128)(2,1)} %param.14) | copy-start | bytes 393220
  7.2 13.6 %copy-start.4 = (f32[8,1,128]{2,1,0:T(1,128)S(1)}, f32[8,1,128]{2,1,0:T(1,128)}, u32[]{:S(2)}) copy-start(f32[8,1,128]{2,1,0:T(1,128)} %param.17) | copy-start | bytes 12292
  7.2 69.9 %copy-start.7 = (bf16[2048,128]{1,0:T(8,128)(2,1)S(1)}, bf16[2048,128]{1,0:T(8,128)(2,1)}, u32[]{:S(2)}) copy-start(bf16[2048,128]{1,0:T(8,128)(2,1)} %param.13) | copy-start | bytes 1572868
  7.2 69.9 %copy-start.8 = (bf16[2048,128]{1,0:T(8,128)(2,1)S(1)}, bf16[2048,128]{1,0:T(8,128)(2,1)}, u32[]{:S(2)}) copy-start(bf16[2048,128]{1,0:T(8,128)(2,1)} %param.12) | copy-start | bytes 1572868
  11.3 61.5 %all-to-all-start = ((bf16[16,8,128,128]{3,2,1,0:T(8,128)(2,1)}), bf16[16,8,128,128]{3,2,1,0:T(8,128)(2,1)}, u32[]{:S(2)}, u32[]{:S(2)}) async-start(bf16[16,8,128,128]{3,2,1,0:T(8,128)(2,1)} %stack.2), calls=%async_computation | async-start | bytes 8388608 | tf_op jit(solution)/shard_map/all_to_all | solution.py:114
  18.9 184.1 %all-gather.5.cloned.1.call-start = ((), (), s32[]{:S(2)}) async-start(), calls=%async_computation.3 | async-start | bytes 1572864 | tf_op jit(solution)/shard_map/all_gather | solution.py:24
  169.3 0.8 copy-start.1
  170.1 142.9 %all-gather.7.cloned.1.call-start = ((), (), s32[]{:S(2)}) async-start(), calls=%async_computation.4 | async-start | bytes 8912896 | tf_op jit(solution)/shard_map/all_gather | solution.py:24
  313.0 10.7 %copy-start.2 = (f32[128,128,128]{2,1,0:T(8,128)S(1)}, f32[128,128,128]{2,1,0:T(8,128)}, u32[]{:S(2)}) copy-start(f32[128,128,128]{2,1,0:T(8,128)} %all-gather.7.cloned.1.call-done) | copy-start | bytes 25165828
  328.4 14.5 %copy-start.5 = (bf16[8,128]{1,0:T(8,128)(2,1)S(1)}, bf16[8,128]{1,0:T(8,128)(2,1)}, u32[]{:S(2)}) copy-start(bf16[8,128]{1,0:T(8,128)(2,1)} %param.18) | copy-start | bytes 6148
  328.4 67.8 %copy-start.6 = (f32[128]{0:T(128)S(1)}, f32[128]{0:T(128)}, u32[]{:S(2)}) copy-start(f32[128]{0:T(128)} %param.19) | copy-start | bytes 1540
  333.1 43.3 %all-to-all-start.1 = ((f32[32,32,128]{2,1,0:T(8,128)}), f32[32,32,128]{2,1,0:T(8,128)S(1)}, u32[]{:S(2)}, u32[]{:S(2)}) async-start(f32[32,32,128]{2,1,0:T(8,128)} %bitcast.33), calls=%async_computation.1 | async-start | bytes 1048576 | tf_op jit(solution)/shard_map/all_to_all | solution.py:42
  376.4 20.4 %copy-start.3 = (bf16[32,128]{1,0:T(8,128)(2,1)}, bf16[32,128]{1,0:T(8,128)(2,1)S(1)}, u32[]{:S(2)}) copy-start(bf16[32,128]{1,0:T(8,128)(2,1)S(1)} %reduce_sum.37) | copy-start | bytes 24580
Sparse Core Ops, SparseCore 0:
  170.2 32.7 all-gather.4
  207.3 105.5 all-gather.6
